TPU v7x, 512 devices: a 4x2x32 block of a 4x8x32 slice. The times are simulated.
512 devices in a mesh: grp: 2 (over y), sp: 32 (over z), tp: 8 (over x, core).
Axes of the slice: x: 4, y: 2, z: 32, core: 2. Of those that a mesh axis runs over, the one named last changes fastest.
The devices are a block of a 4x8x32 slice.
Arguments:
- latent: bfloat16 [32768, 4096], P(('grp', 'sp', 'tp')), parts along dimension 0, may hold values from -260 to 260
- context: bfloat16 [1536, 4096], P(('grp', 'sp')), parts along dimension 0, may hold values from -6 to 6
- conditioning: bfloat16 [8192], P(('grp', 'sp')), parts along dimension 0, may hold values from -6 to 6
- norm_gain: float32 [4096], replicated, may hold values from 0.1 to 1.9
- shift_weight: bfloat16 [4096, 4096], P('sp', 'tp'), may hold values from -0.09375 to 0.09375
- scale_weight: bfloat16 [4096, 4096], P('sp', 'tp'), may hold values from -0.09375 to 0.09375
- gate_weight: bfloat16 [4096, 4096], P('sp', 'tp'), may hold values from -0.09375 to 0.09375
- query_weight: bfloat16 [4096, 1024], P(None, 'tp'), may hold values from -3 to 3
- key_weight: bfloat16 [4096, 512], P(None, 'tp'), may hold values from -3 to 3
- value_weight: bfloat16 [4096, 512], P(None, 'tp'), may hold values from -0.09375 to 0.09375
- out_weight: bfloat16 [1024, 4096], P(None, 'tp'), may hold values from -1.5 to 1.5
- sink_logit: float32 [16], P('tp'), may hold values from 3 to 7
Outputs:
- mixed: bfloat16 [32768, 4096], P(('grp', 'sp', 'tp')), parts along dimension 0
There are 2 independent parts, one for each index of `grp`. A program takes and returns all parts, laid end to end along the dimension named above; an argument that names none is the same for every part. Nothing has to cross between parts.
All inputs are finite; a program needn't handle non-finite values.
Results may differ from a plain program's by a relative error of at most 0.012.
The roundings to bfloat16 on the way count: a program that leaves them out, or rounds other values in their place, can miss the bound.
Values may be sent and summed in bfloat16 or wider, within the bound.
A program may use at most 64 MiB of HBM per device.

v0:
```python
import jax
import jax.numpy as jnp
from jax import lax
from jax.sharding import PartitionSpec as P

HEADS = 16
KV_HEADS = 8
HD = 64
GRID_W = 64
WIN = 128
epsilon = 1e-06
rope_base = 10000.0
neg_large = -1e30


def sent_to_all(value, axis):
    count = lax.axis_size(axis)
    return lax.all_to_all(
        jnp.broadcast_to(value[None], (count, *value.shape)), axis, 0, 0, tiled=True
    )


def over_copies(value, axis):
    return sent_to_all(value, axis).sum(axis=0)


def packed_total(arrays, axis):
    ends = [0]
    for a in arrays:
        ends.append(ends[-1] + a.size)
    running = over_copies(jnp.concatenate([a.ravel() for a in arrays]), axis)
    return tuple((running[b:e].reshape(a.shape) for a, b, e in zip(arrays, ends, ends[1:])))


def rows_first(arrays, axis, dims):
    turned = [jnp.moveaxis(a, dim, 0) for a, dim in zip(arrays, dims)]
    both = jnp.concatenate([t.reshape(len(t), -1) for t in turned], axis=1)
    whole, at, outs = (lax.all_gather(both, axis, axis=0, tiled=True), 0, [])
    for t, dim in zip(turned, dims):
        share = whole[:, at : at + t[0].size].reshape(-1, *t.shape[1:])
        outs.append(jnp.moveaxis(share, 0, dim))
        at += t[0].size
    return tuple(outs)


def with_halo(cells, sides, width):
    for axis, dim in sides:
        count = lax.axis_size(axis)
        ends = count - 1
        head = lax.slice_in_dim(cells, 0, width, axis=dim)
        tail = lax.slice_in_dim(cells, cells.shape[dim] - width, cells.shape[dim], axis=dim)
        cells = jnp.concatenate(
            [
                lax.ppermute(tail, axis, [(i, (i + 1) % count) for i in range(ends)]),
                cells,
                lax.ppermute(head, axis, [((i + 1) % count, i) for i in range(ends)]),
            ],
            axis=dim,
        )
    return cells


def laid_out(tiles, dim):
    shape = list(tiles.shape[1:])
    shape[dim] *= tiles.shape[0]
    return jnp.moveaxis(tiles, 0, dim).reshape(shape)


def collect(value, axis, dim):
    return laid_out(sent_to_all(value, axis), dim)


def row_norm(matrix, norm_gain):
    values = matrix.astype(jnp.float32)
    return (
        values * lax.rsqrt(jnp.mean(values * values, axis=-1, keepdims=True) + epsilon) * norm_gain
    )


def axial_turn(values, position):
    half_dim = values.shape[-1] // 2
    quarter = half_dim // 2
    inverse = rope_base ** (-jnp.arange(quarter, dtype=jnp.float32) / quarter)

    def turn(section, coordinate):
        angles = coordinate.astype(jnp.float32)[:, None] * inverse[None, :]
        cosine = jnp.cos(angles)[:, None, :]
        sine_part = jnp.sin(angles)[:, None, :]
        leading = section[..., :quarter]
        trailing = section[..., quarter:]
        return jnp.concatenate(
            [leading * cosine - trailing * sine_part, leading * sine_part + trailing * cosine],
            axis=-1,
        )

    return jnp.concatenate(
        [
            turn(values[..., :half_dim], position // GRID_W),
            turn(values[..., half_dim:], position % GRID_W),
        ],
        axis=-1,
    )


def context_pairs(context_rows, norm_gain, key_weight, value_weight):
    prepared = row_norm(context_rows, norm_gain).astype(jnp.bfloat16)
    return jnp.concatenate(
        [
            jnp.dot(prepared, key_weight, preferred_element_type=jnp.float32),
            jnp.dot(prepared, value_weight, preferred_element_type=jnp.float32),
        ],
        axis=1,
    ).astype(jnp.bfloat16)


def local(
    latent,
    context,
    conditioning,
    norm_gain,
    shift_weight,
    scale_weight,
    gate_weight,
    query_weight,
    key_weight,
    value_weight,
    out_weight,
    sink_logit,
):
    lifted = jax.nn.silu(conditioning.astype(jnp.float32)).astype(jnp.bfloat16)[None, :]
    shift_part = jnp.dot(lifted, shift_weight, preferred_element_type=jnp.float32)[0]
    scale_part = jnp.dot(lifted, scale_weight, preferred_element_type=jnp.float32)[0]
    gate_part = jnp.dot(lifted, gate_weight, preferred_element_type=jnp.float32)[0]
    summed = packed_total((shift_part, scale_part, gate_part), "sp")
    shift_vec, scale_vec, gate_vec = rows_first((summed[0], summed[1], summed[2]), "tp", (0, 0, 0))
    normed = (row_norm(latent, norm_gain) * (1.0 + scale_vec) + shift_vec).astype(jnp.bfloat16)
    segment = lax.all_gather(normed, "tp", axis=0, tiled=True)
    projected = jnp.concatenate(
        [
            jnp.dot(segment, query_weight, preferred_element_type=jnp.float32),
            jnp.dot(segment, key_weight, preferred_element_type=jnp.float32),
            jnp.dot(segment, value_weight, preferred_element_type=jnp.float32),
        ],
        axis=1,
    )
    row_count = projected.shape[0]
    query_width = query_weight.shape[1]
    key_width = key_weight.shape[1]
    query_heads = query_width // HD
    pair_heads = key_width // HD
    group_size = HEADS // KV_HEADS
    row_offset = lax.axis_index("sp") * row_count
    position = row_offset + jnp.arange(row_count, dtype=jnp.int32)
    queries = axial_turn(
        projected[:, :query_width].reshape(row_count, query_heads, HD), position
    ).astype(jnp.bfloat16)
    latent_keys = axial_turn(
        projected[:, query_width : query_width + key_width].reshape(row_count, pair_heads, HD),
        position,
    ).astype(jnp.bfloat16)
    latent_values = projected[:, query_width + key_width :].astype(jnp.bfloat16)
    key_value = jnp.concatenate([latent_keys.reshape(row_count, key_width), latent_values], axis=1)
    widened = with_halo(key_value, (("sp", 0),), WIN)
    context_all = collect(context_pairs(context, norm_gain, key_weight, value_weight), "sp", 0)
    block_count = row_count // WIN
    context_count = context_all.shape[0]
    query_blocks = queries.reshape(block_count, WIN, pair_heads, group_size, HD)
    band_blocks = widened.reshape(block_count + 2, WIN, 2 * key_width)
    band_rows = jnp.concatenate(
        [band_blocks[:block_count], band_blocks[1 : block_count + 1], band_blocks[2:]], axis=1
    )
    band_keys = band_rows[..., :key_width].reshape(block_count, 3 * WIN, pair_heads, HD)
    band_values = band_rows[..., key_width:].reshape(block_count, 3 * WIN, pair_heads, HD)
    context_keys = context_all[:, :key_width].reshape(context_count, pair_heads, HD)
    context_values = context_all[:, key_width:].reshape(context_count, pair_heads, HD)
    factor = HD ** (-0.5)
    local_scores = (
        jnp.einsum("nqhgd,nkhd->nhgqk", query_blocks, band_keys, preferred_element_type=jnp.float32)
        * factor
    )
    query_pos = position.reshape(block_count, WIN)
    key_pos = (
        row_offset
        - WIN
        + jnp.arange(block_count, dtype=jnp.int32)[:, None] * WIN
        + jnp.arange(3 * WIN, dtype=jnp.int32)[None, :]
    )
    seq_total = row_count * lax.axis_size("sp")
    allowed = (
        (jnp.abs(key_pos[:, None, :] - query_pos[:, :, None]) <= WIN)
        & (key_pos[:, None, :] >= 0)
        & (key_pos[:, None, :] < seq_total)
    )
    local_scores = jnp.where(allowed[:, None, None], local_scores, neg_large)
    context_scores = (
        jnp.einsum(
            "nqhgd,thd->nhgqt", query_blocks, context_keys, preferred_element_type=jnp.float32
        )
        * factor
    )
    sink_values = sink_logit.reshape(pair_heads, group_size)[None, :, :, None, None]
    highest = jnp.maximum(
        jnp.maximum(
            jnp.max(local_scores, axis=-1, keepdims=True),
            jnp.max(context_scores, axis=-1, keepdims=True),
        ),
        sink_values,
    )
    local_exp = jnp.exp(local_scores - highest)
    context_exp = jnp.exp(context_scores - highest)
    denominator = (
        jnp.sum(local_exp, axis=-1, keepdims=True)
        + jnp.sum(context_exp, axis=-1, keepdims=True)
        + jnp.exp(sink_values - highest)
    )
    local_weights = (local_exp / denominator).astype(jnp.bfloat16)
    context_weights = (context_exp / denominator).astype(jnp.bfloat16)
    attended = jnp.einsum(
        "nhgqk,nkhd->nqhgd", local_weights, band_values, preferred_element_type=jnp.float32
    ) + jnp.einsum(
        "nhgqt,thd->nqhgd", context_weights, context_values, preferred_element_type=jnp.float32
    )
    attended = attended.reshape(row_count, query_width).astype(jnp.bfloat16)
    columns_part = jnp.dot(
        collect(attended, "tp", 1), out_weight, preferred_element_type=jnp.float32
    ).astype(jnp.bfloat16)
    blended = lax.all_to_all(columns_part, "tp", split_axis=0, concat_axis=1, tiled=True)
    return (latent.astype(jnp.float32) + gate_vec * blended.astype(jnp.float32)).astype(
        jnp.bfloat16
    )


def solution(mesh):
    in_specs = (
        P(("grp", "sp", "tp"), None),
        P(("grp", "sp"), None),
        P(("grp", "sp")),
        P(),
        P("sp", "tp"),
        P("sp", "tp"),
        P("sp", "tp"),
        P(None, "tp"),
        P(None, "tp"),
        P(None, "tp"),
        P(None, "tp"),
        P("tp"),
    )
    out_specs = P(("grp", "sp", "tp"), None)
    return jax.shard_map(local, mesh=mesh, in_specs=in_specs, out_specs=out_specs, check_vma=False)
```

profile of v0, /device:TPU:33, one launch (start us, length us, event | category | flops | bytes accessed | tf_op | source)
XLA Modules:
  0.0 197.6 jit_solution(16965403692785830598)
XLA Ops:
  6.5 0.0 copy-start
  6.6 1.2 fusion.60
  7.8 1.1 fusion.58
  8.8 1.1 fusion.56
  9.9 0.8 broadcast_in_dim.14
  10.7 46.3 %all-to-all-start = ((f32[32,1,1536]{2,1,0:T(1,128)}), f32[32,1,1536]{2,1,0:T(1,128)S(1)}, u32[]{:S(2)}, u32[]{:S(2)}) async-start(f32[32,1,1536]{2,1,0:T(1,128)} %broadcast_in_dim.14), calls=%async_computation | async-start | bytes 393216 | tf_op jit(solution)/shard_map/all_to_all | solution.py:18
  57.0 0.1 all-gather.2.cloned.1.call-start
  57.1 1.2 fusion.12
  58.3 33.6 %all-to-all-done = f32[32,1,1536]{2,1,0:T(1,128)S(1)} async-done(((f32[32,1,1536]{2,1,0:T(1,128)}), f32[32,1,1536]{2,1,0:T(1,128)S(1)}, u32[]{:S(2)}, u32[]{:S(2)}) %all-to-all-start) | async-done | bytes 196640 | tf_op jit(solution)/shard_map/all_to_all | solution.py:18
  91.9 0.1 reduce_sum.45
  92.0 15.7 %all_gather.6 = f32[4096,3]{0,1:T(4,128)S(1)} all-gather(f32[512,3]{0,1:T(4,128)S(1)} %pad_maximum_fusion.3), channel_id=1, replica_groups=mesh['grp'=2,'sp'=32,'tp'=8] {'tp'}, dimensions={0}, use_global_device_ids=true | all-gather | bytes 55296 | tf_op jit(solution)/shard_map/all_gather | solution.py:38
  107.8 2.1 %fusion.16 = bf16[64,4096]{1,0:T(8,128)(2,1)} fusion(bf16[64,4096]{1,0:T(8,128)(2,1)} %param.12, f32[4096]{0:T(1024)S(1)} %bitcast.164, f32[4096]{0:T(1024)S(1)} %bitcast.165, f32[4096]{0:T(1024)} %param.15, f32[64]{0:T(128)S(1)} %add_rsqrt_fusion.1), kind=kLoop, calls=%fused_computation.29 | loop fusion | flops 1572864 | bytes 1097984 | tf_op jit(solution)/shard_map/convert_element_type | solution.py:136
  109.9 0.1 all-gather.2.cloned.1.call-update
  110.0 0.0 copy-done.5
  110.0 0.2 fusion.21
  110.2 0.0 copy-done.7
  110.2 0.0 copy-done.4
  110.2 0.3 convolution_convert_fusion.2
  110.5 0.0 copy-done.3
  110.5 0.3 convolution_convert_fusion.3
  110.8 0.1 pad_maximum_fusion.4
  110.9 0.7 broadcast_in_dim.17
  111.6 4.8 %all-to-all-start.1 = ((bf16[32,24,128]{2,1,0:T(8,128)(2,1)}), bf16[32,24,128]{2,1,0:T(8,128)(2,1)S(1)}, u32[]{:S(2)}, u32[]{:S(2)}) async-start(bf16[32,24,128]{2,1,0:T(8,128)(2,1)} %broadcast_in_dim.17), calls=%async_computation.1 | async-start | bytes 393216 | tf_op jit(solution)/shard_map/all_to_all | solution.py:18
  116.5 0.1 fusion.50
  116.5 0.1 iota_add_fusion
  116.6 0.3 multiply_cosine_fusion
  116.9 0.9 fusion.20
  117.9 21.9 %all-gather.2.cloned.1.call-done = bf16[512,4096]{1,0:T(8,128)(2,1)} async-done(((bf16[64,4096]{1,0:T(8,128)(2,1)}), bf16[512,4096]{1,0:T(8,128)(2,1)}) %all-gather.2.cloned.1.call-update) | async-done | bytes 4194320 | tf_op jit(solution)/shard_map/all_gather | solution.py:137
  139.8 3.7 %convolution_bitcast_fusion.1 = f32[512,1,64]{0,2,1:T(8,128)S(1)} fusion(bf16[512,4096]{1,0:T(8,128)(2,1)} %all-gather.2.cloned.1.call-done, bf16[4096,64]{0,1:T(8,128)(2,1)S(1)} %copy-done.3), kind=kOutput, calls=%fused_computation.20 | convolution fusion | flops 268435456 | bytes 4849664 | tf_op jit(solution)/shard_map/dot_general | solution.py:141
  143.5 0.0 copy-start.6
  143.5 0.2 constant_dynamic-update-slice_fusion.3
  143.7 0.2 constant_dynamic-update-slice_fusion.2
  143.9 0.2 constant_dynamic-update-slice_fusion.1
  144.1 0.2 constant_dynamic-update-slice_fusion
  144.3 0.0 copy-done.1
  144.3 1.4 fusion.11
  145.7 1.3 collective-permute-start.1
  147.0 4.2 %collective-permute-start = (bf16[128,128]{0,1:T(8,128)(2,1)S(1)}, bf16[128,128]{0,1:T(8,128)(2,1)S(1)}, u32[]{:S(2)}, u32[]{:S(2)}) collective-permute-start(bf16[128,128]{0,1:T(8,128)(2,1)S(1)} %get-tuple-element.14), channel_id=1, source_target_pairs={{0,8},{8,16},{16,24},{24,32},{32,40},{40,48},{48,56},{56,64},{64,7... | collective-permute-start | bytes 98312 | tf_op jit(solution)/shard_map/ppermute | solution.py:54
  151.2 0.0 copy-done.6
  151.3 1.5 fusion.70
  152.9 0.0 all-to-all-done.1
  152.9 0.0 copy-start.8
  152.9 0.6 bitcast_reduce_fusion
  153.5 0.0 collective-permute-done.1
  153.5 0.0 collective-permute-done
  153.7 0.4 fusion.69
  154.1 0.0 copy-done.8
  154.1 0.1 maximum_maximum_fusion
  154.2 0.5 fusion.1
  154.8 0.2 fusion.5
  155.0 0.1 exponential_add_fusion
  155.1 0.8 fusion.7
  155.9 0.4 fusion.10
  156.3 0.1 copy.58
  156.4 0.1 broadcast_in_dim.18
  156.5 19.3 %all_to_all.29 = bf16[8,512,128]{1,2,0:T(8,128)(2,1)S(1)} all-to-all(bf16[8,512,128]{1,2,0:T(8,128)(2,1)S(1)} %broadcast_in_dim.18), channel_id=1, replica_groups=mesh['grp'=2,'sp'=32,'tp'=8] {'tp'}, dimensions={0} | all-to-all | bytes 2097152 | tf_op jit(solution)/shard_map/all_to_all | solution.py:18
  175.9 0.0 copy-done
  175.9 0.7 convolution_convert_fusion
  176.6 0.0 copy-start.2
  176.6 13.0 %all_to_all.30 = bf16[8,64,512]{2,1,0:T(8,128)(2,1)S(1)} all-to-all(bf16[8,64,512]{2,1,0:T(8,128)(2,1)S(1)} %bitcast.161), channel_id=1, replica_groups=mesh['grp'=2,'sp'=32,'tp'=8] {'tp'}, dimensions={0} | all-to-all | bytes 1048576 | tf_op jit(solution)/shard_map/all_to_all | solution.py:227
  189.6 0.1 convert_bitcast_fusion
  189.7 0.1 copy.79
  189.8 0.0 copy-done.2
  189.8 0.9 fusion.17
  (26 shorter events, 0.4 us)
Async XLA Ops:
  6.5 169.3 %copy-start = (bf16[1024,512]{1,0:T(8,128)(2,1)S(1)}, bf16[1024,512]{1,0:T(8,128)(2,1)}, u32[]{:S(2)}) copy-start(bf16[1024,512]{1,0:T(8,128)(2,1)} %param.22) | copy-start | bytes 3145732
  6.6 103.6 %copy-start.7 = (f32[4096]{0:T(1024)S(1)}, f32[4096]{0:T(1024)}, u32[]{:S(2)}) copy-start(f32[4096]{0:T(1024)} %param.15) | copy-start | bytes 49156
  6.6 103.4 %copy-start.5 = (bf16[24,4096]{1,0:T(8,128)(2,1)S(1)}, bf16[24,4096]{1,0:T(8,128)(2,1)}, u32[]{:S(2)}) copy-start(bf16[24,4096]{1,0:T(8,128)(2,1)} %param.13) | copy-start | bytes 589828
  6.6 103.6 %copy-start.4 = (bf16[4096,64]{0,1:T(8,128)(2,1)S(1)}, bf16[4096,64]{0,1:T(8,128)(2,1)}, u32[]{:S(2)}) copy-start(bf16[4096,64]{0,1:T(8,128)(2,1)} %param.21) | copy-start | bytes 1572868
  6.6 103.9 %copy-start.3 = (bf16[4096,64]{0,1:T(8,128)(2,1)S(1)}, bf16[4096,64]{0,1:T(8,128)(2,1)}, u32[]{:S(2)}) copy-start(bf16[4096,64]{0,1:T(8,128)(2,1)} %param.20) | copy-start | bytes 1572868
  10.7 81.2 %all-to-all-start = ((f32[32,1,1536]{2,1,0:T(1,128)}), f32[32,1,1536]{2,1,0:T(1,128)S(1)}, u32[]{:S(2)}, u32[]{:S(2)}) async-start(f32[32,1,1536]{2,1,0:T(1,128)} %broadcast_in_dim.14), calls=%async_computation | async-start | bytes 393216 | tf_op jit(solution)/shard_map/all_to_all | solution.py:18
  57.0 82.8 %all-gather.2.cloned.1.call-start = ((), (), s32[]{:S(2)}) async-start(), calls=%async_computation.4 | async-start | bytes 4718592 | tf_op jit(solution)/shard_map/all_gather | solution.py:137
  111.6 41.3 %all-to-all-start.1 = ((bf16[32,24,128]{2,1,0:T(8,128)(2,1)}), bf16[32,24,128]{2,1,0:T(8,128)(2,1)S(1)}, u32[]{:S(2)}, u32[]{:S(2)}) async-start(bf16[32,24,128]{2,1,0:T(8,128)(2,1)} %broadcast_in_dim.17), calls=%async_computation.1 | async-start | bytes 393216 | tf_op jit(solution)/shard_map/all_to_all | solution.py:18
  139.8 4.5 %copy-start.1 = (bf16[512,4096]{1,0:T(8,128)(2,1)S(1)}, bf16[512,4096]{1,0:T(8,128)(2,1)}, u32[]{:S(2)}) copy-start(bf16[512,4096]{1,0:T(8,128)(2,1)} %all-gather.2.cloned.1.call-done) | copy-start | bytes 12582916
  143.5 7.8 %copy-start.6 = (bf16[4096,128]{1,0:T(8,128)(2,1)S(1)}, bf16[4096,128]{1,0:T(8,128)(2,1)}, u32[]{:S(2)}) copy-start(bf16[4096,128]{1,0:T(8,128)(2,1)} %param.19) | copy-start | bytes 3145732
  145.7 7.8 %collective-permute-start.1 = (bf16[128,128]{0,1:T(8,128)(2,1)S(1)}, bf16[128,128]{0,1:T(8,128)(2,1)S(1)}, u32[]{:S(2)}, u32[]{:S(2)}) collective-permute-start(bf16[128,128]{0,1:T(8,128)(2,1)S(1)} %get-tuple-element.13), channel_id=1, source_target_pairs={{8,0},{16,8},{24,16},{32,24},{40,32},{48,40},{56,48},{64,56},{72,6... | collective-permute-start | bytes 98312 | tf_op jit(solution)/shard_map/ppermute | solution.py:56
  147.0 6.5 %collective-permute-start = (bf16[128,128]{0,1:T(8,128)(2,1)S(1)}, bf16[128,128]{0,1:T(8,128)(2,1)S(1)}, u32[]{:S(2)}, u32[]{:S(2)}) collective-permute-start(bf16[128,128]{0,1:T(8,128)(2,1)S(1)} %get-tuple-element.14), channel_id=1, source_target_pairs={{0,8},{8,16},{16,24},{24,32},{32,40},{40,48},{48,56},{56,64},{64,7... | collective-permute-start | bytes 98312 | tf_op jit(solution)/shard_map/ppermute | solution.py:54
  152.9 1.2 copy-start.8
  176.6 13.2 %copy-start.2 = (bf16[64,4096]{1,0:T(8,128)(2,1)S(1)}, bf16[64,4096]{1,0:T(8,128)(2,1)}, u32[]{:S(2)}) copy-start(bf16[64,4096]{1,0:T(8,128)(2,1)} %param.12) | copy-start | bytes 1572868
Sparse Core Ops, SparseCore 0:
  110.1 29.6 all-gather.1
where the time goes:
time: 198 us
  starting transfers between devices  56.7 us (29%)
  waiting for transfers between devices  55.5 us (28%)
  blocking collectives  48 us (24%)
  between operations  13.8 us (7%)
  matrix products  13.5 us (7%)
  other arithmetic  8.05 us (4%)
  local copies, waits for them, and re-layouts  2.02 us (1%)
    all_to_all x2, starting transfers between devices, sent_to_all(): lax.all_to_all(jnp.broadcast_to(value[None], (count, *value.shape)), axis...  51.1 us
    all_to_all x2, waiting for transfers between devices, sent_to_all(): lax.all_to_all(jnp.broadcast_to(value[None], (count, *value.shape)), axis...  33.6 us
    all_gather x1, waiting for transfers between devices, local(): segment = lax.all_gather(normed, 'tp', axis=0, tiled=True)  21.9 us
    all_to_all x1, blocking collectives, sent_to_all(): lax.all_to_all(jnp.broadcast_to(value[None], (count, *value.shape)), axis...  19.3 us
    all_gather x1, blocking collectives, rows_first(): whole, at, outs = (lax.all_gather(both, axis, axis=0, tiled=True), 0, [])  15.7 us
    all_to_all x1, blocking collectives, local(): lax.all_to_all(columns_part, 'tp', split_axis=0, concat_axis=1, tiled=True)  13 us
    ppermute x1, starting transfers between devices, with_halo(): lax.ppermute(tail, axis, [(i, (i + 1) % count) for i in range(ends)])  4.21 us
  transfers between devices with their start and end apart: 5, of which 2 were waited for; matrix products, arithmetic and copies ran while one was open for 6% of the time, Pallas kernels for 0%

commit v1 on v0

--- a/solution.py
+++ b/solution.py
@@ -134,7 +134,9 @@
     summed = packed_total((shift_part, scale_part, gate_part), "sp")
     shift_vec, scale_vec, gate_vec = rows_first((summed[0], summed[1], summed[2]), "tp", (0, 0, 0))
     normed = (row_norm(latent, norm_gain) * (1.0 + scale_vec) + shift_vec).astype(jnp.bfloat16)
-    segment = lax.all_gather(normed, "tp", axis=0, tiled=True)
+    segment = jnp.concatenate(
+        lax.all_to_all(jnp.stack([normed] * lax.axis_size("tp")), "tp", 0, 0), axis=0
+    )
     projected = jnp.concatenate(
         [
             jnp.dot(segment, query_weight, preferred_element_type=jnp.float32),

time: 198 us -> 238 us (1.20)
  waiting for transfers between devices: 55.5 us -> 97.3 us
  between operations: 13.8 us -> 0.37 us
  matrix products: 13.5 us -> 17.7 us
  local copies, waits for them, and re-layouts: 2.02 us -> 5.89 us
  starting transfers between devices: 56.7 us -> 59.7 us
    all_to_all x0 -> x1, waiting for transfers between devices: none -> 45.1 us  [local(): lax.all_to_all(jnp.stack([normed] * lax.axis_size('tp')), 'tp', 0, 0)]
    all_gather x1 -> x0, waiting for transfers between devices: 21.9 us -> none  [local(): segment = lax.all_gather(normed, 'tp', axis=0, tiled=True)]
    all_to_all x2, waiting for transfers between devices: 33.6 us -> 52.2 us  [sent_to_all(): lax.all_to_all(jnp.broadcast_to(value[None], (count, *value.shape)), axis...]
    all_to_all x0 -> x1, starting transfers between devices: none -> 4.75 us  [local(): lax.all_to_all(jnp.stack([normed] * lax.axis_size('tp')), 'tp', 0, 0)]
    another operation x0 -> x1, local copies, waits for them, and re-layouts: none -> 2.5 us  [local(): jnp.stack([normed] * lax.axis_size('tp'))]
  transfers between devices with their start and end apart: 5 -> 5, of which waited for: 2 -> 3; matrix products, arithmetic and copies ran while one was open for 6% -> 7% of each run, Pallas kernels for 0% -> 0%
where the time goes in v1:
time: 238 us
  waiting for transfers between devices  97.3 us (41%)
  starting transfers between devices  59.7 us (25%)
  blocking collectives  49.4 us (21%)
  matrix products  17.7 us (7%)
  other arithmetic  7.25 us (3%)
  local copies, waits for them, and re-layouts  5.89 us (2%)
    all_to_all x2, waiting for transfers between devices, sent_to_all(): lax.all_to_all(jnp.broadcast_to(value[None], (count, *value.shape)), axis...  52.2 us
    all_to_all x2, starting transfers between devices, sent_to_all(): lax.all_to_all(jnp.broadcast_to(value[None], (count, *value.shape)), axis...  51.1 us
    all_to_all x1, waiting for transfers between devices, local(): lax.all_to_all(jnp.stack([normed] * lax.axis_size('tp')), 'tp', 0, 0)  45.1 us
    all_to_all x1, blocking collectives, sent_to_all(): lax.all_to_all(jnp.broadcast_to(value[None], (count, *value.shape)), axis...  20.7 us
    all_gather x1, blocking collectives, rows_first(): whole, at, outs = (lax.all_gather(both, axis, axis=0, tiled=True), 0, [])  15.7 us
    all_to_all x1, blocking collectives, local(): lax.all_to_all(columns_part, 'tp', split_axis=0, concat_axis=1, tiled=True)  13 us
  transfers between devices with their start and end apart: 5, of which 3 were waited for; matrix products, arithmetic and copies ran while one was open for 7% of the time, Pallas kernels for 0%

profile of v1, /device:TPU:33, one launch (start us, length us, event | category | flops | bytes accessed | tf_op | source)
XLA Modules:
  0.0 237.6 jit_solution(15978489735749285395)
XLA Ops:
  0.0 0.0 copy-start
  0.0 1.1 fusion.60
  1.1 1.1 fusion.58
  2.2 1.1 fusion.56
  3.3 0.8 broadcast_in_dim.14
  4.1 46.3 %all-to-all-start = ((f32[32,1,1536]{2,1,0:T(1,128)}), f32[32,1,1536]{2,1,0:T(1,128)S(1)}, u32[]{:S(2)}, u32[]{:S(2)}) async-start(f32[32,1,1536]{2,1,0:T(1,128)} %broadcast_in_dim.14), calls=%async_computation | async-start | bytes 393216 | tf_op jit(solution)/shard_map/all_to_all | solution.py:18
  50.4 1.2 fusion.12
  51.6 33.6 %all-to-all-done = f32[32,1,1536]{2,1,0:T(1,128)S(1)} async-done(((f32[32,1,1536]{2,1,0:T(1,128)}), f32[32,1,1536]{2,1,0:T(1,128)S(1)}, u32[]{:S(2)}, u32[]{:S(2)}) %all-to-all-start) | async-done | bytes 196640 | tf_op jit(solution)/shard_map/all_to_all | solution.py:18
  85.3 0.1 reduce_sum.45
  85.4 15.7 %all_gather.3 = f32[4096,3]{0,1:T(4,128)S(1)} all-gather(f32[512,3]{0,1:T(4,128)S(1)} %pad_maximum_fusion.3), channel_id=1, replica_groups=mesh['grp'=2,'sp'=32,'tp'=8] {'tp'}, dimensions={0}, use_global_device_ids=true | all-gather | bytes 55296 | tf_op jit(solution)/shard_map/all_gather | solution.py:38
  101.2 1.3 fusion.16
  102.5 2.5 %stack.2 = bf16[8,64,4096]{2,1,0:T(8,128)(2,1)} broadcast(bf16[64,4096]{1,0:T(8,128)(2,1)S(1)} %fusion.16), dimensions={1,2} | broadcast | bytes 4718592 | tf_op jit(solution)/shard_map/stack | solution.py:138
  105.0 0.0 copy-start.2
  105.0 4.8 %all-to-all-start.1 = ((bf16[8,64,4096]{2,1,0:T(8,128)(2,1)}), bf16[8,64,4096]{2,1,0:T(8,128)(2,1)}, u32[]{:S(2)}, u32[]{:S(2)}) async-start(bf16[8,64,4096]{2,1,0:T(8,128)(2,1)} %stack.2), calls=%async_computation.1 | async-start | bytes 8388608 | tf_op jit(solution)/shard_map/all_to_all | solution.py:138
  109.8 0.0 copy-done.5
  109.8 1.4 copy.57
  111.2 0.0 copy-done.4
  111.2 0.2 fusion.21
  111.4 0.0 copy-done.3
  111.4 0.0 copy-done.7
  111.4 0.3 convolution_convert_fusion.2
  111.7 0.0 copy-done.2
  111.7 0.3 convolution_convert_fusion.3
  112.1 0.1 pad_maximum_fusion.4
  112.1 0.1 fusion.50
  112.2 0.1 iota_add_fusion
  112.3 0.3 multiply_cosine_fusion
  112.6 0.9 fusion.20
  113.6 45.1 %all-to-all-done.1 = bf16[8,64,4096]{2,1,0:T(8,128)(2,1)} async-done(((bf16[8,64,4096]{2,1,0:T(8,128)(2,1)}), bf16[8,64,4096]{2,1,0:T(8,128)(2,1)}, u32[]{:S(2)}, u32[]{:S(2)}) %all-to-all-start.1) | async-done | bytes 4194336 | tf_op jit(solution)/shard_map/all_to_all | solution.py:138
  158.7 0.7 broadcast_in_dim.17
  159.4 4.8 %all-to-all-start.2 = ((bf16[32,24,128]{2,1,0:T(8,128)(2,1)}), bf16[32,24,128]{2,1,0:T(8,128)(2,1)S(1)}, u32[]{:S(2)}, u32[]{:S(2)}) async-start(bf16[32,24,128]{2,1,0:T(8,128)(2,1)} %broadcast_in_dim.17), calls=%async_computation.2 | async-start | bytes 393216 | tf_op jit(solution)/shard_map/all_to_all | solution.py:18
  164.1 3.6 %convolution_bitcast_fusion.1 = f32[512,1,64]{0,2,1:T(8,128)S(1)} fusion(bf16[512,4096]{1,0:T(8,128)(2,1)} %bitcast.12, bf16[4096,64]{0,1:T(8,128)(2,1)S(1)} %copy-done.2), kind=kOutput, calls=%fused_computation.20 | convolution fusion | flops 268435456 | bytes 4849664 | tf_op jit(solution)/shard_map/dot_general | solution.py:143
  167.7 0.2 constant_dynamic-update-slice_fusion.3
  167.9 0.2 constant_dynamic-update-slice_fusion.2
  168.1 0.2 constant_dynamic-update-slice_fusion.1
  168.3 0.2 constant_dynamic-update-slice_fusion
  168.5 3.6 %fusion.11 = bf16[512,128]{0,1:T(8,128)(2,1)S(1)} fusion(bf16[512,128]{0,1:T(8,128)(2,1)S(1)} %constant_dynamic-update-slice_fusion, bf16[512,4096]{1,0:T(8,128)(2,1)} %bitcast.12, bf16[4096,64]{0,1:T(8,128)(2,1)S(1)} %copy-done.3), kind=kOutput, calls=%fused_computation.22 | convolution fusion | flops 268468224 | bytes 4784128 | tf_op jit(solution)/shard_map/dot_general | solution.py:144
  172.1 2.4 collective-permute-start
  174.5 1.5 collective-permute-start.1
  176.0 0.0 copy-done.6
  176.0 3.7 %fusion.70 = f32[512,2,64]{0,2,1:T(8,128)S(1)} fusion(bf16[512,4096,1]{1,0,2:T(8,128)(2,1)} %bitcast.22, bf16[2,64,4096]{2,1,0:T(8,128)(2,1)S(1)} %bitcast.161), kind=kOutput, calls=%fused_computation.135 | convolution fusion | flops 536870912 | bytes 5505024 | tf_op jit(solution)/shard_map/dot_general | solution.py:142
  179.9 18.6 %all-to-all-done.2 = bf16[32,24,128]{2,1,0:T(8,128)(2,1)S(1)} async-done(((bf16[32,24,128]{2,1,0:T(8,128)(2,1)}), bf16[32,24,128]{2,1,0:T(8,128)(2,1)S(1)}, u32[]{:S(2)}, u32[]{:S(2)}) %all-to-all-start.2) | async-done | bytes 196640 | tf_op jit(solution)/shard_map/all_to_all | solution.py:18
  198.4 0.6 bitcast_reduce_fusion
  199.0 0.0 collective-permute-done
  199.0 0.0 collective-permute-done.1
  199.2 0.4 fusion.69
  199.6 0.0 copy-done.8
  199.6 0.1 maximum_maximum_fusion
  199.7 0.5 fusion.1
  200.2 0.2 fusion.5
  200.5 0.1 exponential_add_fusion
  200.6 0.8 fusion.7
  201.4 0.4 fusion.10
  201.8 0.1 copy.66
  201.9 0.1 broadcast_in_dim.18
  202.0 20.7 %all_to_all.34 = bf16[8,512,128]{1,2,0:T(8,128)(2,1)S(1)} all-to-all(bf16[8,512,128]{1,2,0:T(8,128)(2,1)S(1)} %broadcast_in_dim.18), channel_id=1, replica_groups=mesh['grp'=2,'sp'=32,'tp'=8] {'tp'}, dimensions={0} | all-to-all | bytes 2097152 | tf_op jit(solution)/shard_map/all_to_all | solution.py:18
  222.7 0.0 copy-done
  222.7 0.7 convolution_convert_fusion
  223.4 0.0 copy-start.1
  223.5 13.0 %all_to_all.35 = bf16[8,64,512]{2,1,0:T(8,128)(2,1)S(1)} all-to-all(bf16[8,64,512]{2,1,0:T(8,128)(2,1)S(1)} %bitcast.166), channel_id=1, replica_groups=mesh['grp'=2,'sp'=32,'tp'=8] {'tp'}, dimensions={0} | all-to-all | bytes 1048576 | tf_op jit(solution)/shard_map/all_to_all | solution.py:229
  236.4 0.1 convert_bitcast_fusion
  236.6 0.1 copy.87
  236.7 0.0 copy-done.1
  236.7 0.9 fusion.17
  (27 shorter events, 0.4 us)
Async XLA Ops:
  0.0 222.7 %copy-start = (bf16[1024,512]{1,0:T(8,128)(2,1)S(1)}, bf16[1024,512]{1,0:T(8,128)(2,1)}, u32[]{:S(2)}) copy-start(bf16[1024,512]{1,0:T(8,128)(2,1)} %param.22) | copy-start | bytes 3145732
  4.1 81.2 %all-to-all-start = ((f32[32,1,1536]{2,1,0:T(1,128)}), f32[32,1,1536]{2,1,0:T(1,128)S(1)}, u32[]{:S(2)}, u32[]{:S(2)}) async-start(f32[32,1,1536]{2,1,0:T(1,128)} %broadcast_in_dim.14), calls=%async_computation | async-start | bytes 393216 | tf_op jit(solution)/shard_map/all_to_all | solution.py:18
  105.0 4.8 %copy-start.5 = (bf16[4096,128]{1,0:T(8,128)(2,1)S(1)}, bf16[4096,128]{1,0:T(8,128)(2,1)}, u32[]{:S(2)}) copy-start(bf16[4096,128]{1,0:T(8,128)(2,1)} %param.19) | copy-start | bytes 3145732
  105.0 6.2 %copy-start.4 = (bf16[24,4096]{1,0:T(8,128)(2,1)S(1)}, bf16[24,4096]{1,0:T(8,128)(2,1)}, u32[]{:S(2)}) copy-start(bf16[24,4096]{1,0:T(8,128)(2,1)} %param.13) | copy-start | bytes 589828
  105.0 6.4 %copy-start.3 = (bf16[4096,64]{0,1:T(8,128)(2,1)S(1)}, bf16[4096,64]{0,1:T(8,128)(2,1)}, u32[]{:S(2)}) copy-start(bf16[4096,64]{0,1:T(8,128)(2,1)} %param.21) | copy-start | bytes 1572868
  105.0 6.4 %copy-start.7 = (f32[4096]{0:T(1024)S(1)}, f32[4096]{0:T(1024)}, u32[]{:S(2)}) copy-start(f32[4096]{0:T(1024)} %param.15) | copy-start | bytes 49156
  105.0 6.7 %copy-start.2 = (bf16[4096,64]{0,1:T(8,128)(2,1)S(1)}, bf16[4096,64]{0,1:T(8,128)(2,1)}, u32[]{:S(2)}) copy-start(bf16[4096,64]{0,1:T(8,128)(2,1)} %param.20) | copy-start | bytes 1572868
  105.0 53.6 %all-to-all-start.1 = ((bf16[8,64,4096]{2,1,0:T(8,128)(2,1)}), bf16[8,64,4096]{2,1,0:T(8,128)(2,1)}, u32[]{:S(2)}, u32[]{:S(2)}) async-start(bf16[8,64,4096]{2,1,0:T(8,128)(2,1)} %stack.2), calls=%async_computation.1 | async-start | bytes 8388608 | tf_op jit(solution)/shard_map/all_to_all | solution.py:138
  159.4 39.1 %all-to-all-start.2 = ((bf16[32,24,128]{2,1,0:T(8,128)(2,1)}), bf16[32,24,128]{2,1,0:T(8,128)(2,1)S(1)}, u32[]{:S(2)}, u32[]{:S(2)}) async-start(bf16[32,24,128]{2,1,0:T(8,128)(2,1)} %broadcast_in_dim.17), calls=%async_computation.2 | async-start | bytes 393216 | tf_op jit(solution)/shard_map/all_to_all | solution.py:18
  167.7 8.3 %copy-start.6 = (bf16[4096,128]{0,1:T(8,128)(2,1)S(1)}, bf16[4096,128]{0,1:T(8,128)(2,1)}, u32[]{:S(2)}) copy-start(bf16[4096,128]{0,1:T(8,128)(2,1)} %copy.57) | copy-start | bytes 3145732
  172.1 26.9 %collective-permute-start = (bf16[128,128]{0,1:T(8,128)(2,1)S(1)}, bf16[128,128]{0,1:T(8,128)(2,1)S(1)}, u32[]{:S(2)}, u32[]{:S(2)}) collective-permute-start(bf16[128,128]{0,1:T(8,128)(2,1)S(1)} %get-tuple-element.14), channel_id=1, source_target_pairs={{0,8},{8,16},{16,24},{24,32},{32,40},{40,48},{48,56},{56,64},{64,7... | collective-permute-start | bytes 98312 | tf_op jit(solution)/shard_map/ppermute | solution.py:54
  174.5 24.5 %collective-permute-start.1 = (bf16[128,128]{0,1:T(8,128)(2,1)S(1)}, bf16[128,128]{0,1:T(8,128)(2,1)S(1)}, u32[]{:S(2)}, u32[]{:S(2)}) collective-permute-start(bf16[128,128]{0,1:T(8,128)(2,1)S(1)} %get-tuple-element.13), channel_id=1, source_target_pairs={{8,0},{16,8},{24,16},{32,24},{40,32},{48,40},{56,48},{64,56},{72,6... | collective-permute-start | bytes 98312 | tf_op jit(solution)/shard_map/ppermute | solution.py:56
  198.4 1.2 copy-start.8
  223.4 13.2 %copy-start.1 = (bf16[64,4096]{1,0:T(8,128)(2,1)S(1)}, bf16[64,4096]{1,0:T(8,128)(2,1)}, u32[]{:S(2)}) copy-start(bf16[64,4096]{1,0:T(8,128)(2,1)} %param.12) | copy-start | bytes 1572868
